TPU v7x, 32 devices: a whole 2x2x4 slice. The times are simulated.
32 devices in a mesh: ep: 8 (over z, y), tp: 4 (over x, core).
Axes of the slice: x: 2, y: 2, z: 4, core: 2. Of those that a mesh axis runs over, the one named last changes fastest.
Arguments:
- tokens: bfloat16 [64, 2048], P('ep'), may hold values from -4 to 4
- w_query: bfloat16 [2048, 1024], P(None, 'tp'), may hold values from -0.125 to 0.125
- w_key: bfloat16 [2048, 1024], P(None, 'tp'), may hold values from -0.125 to 0.125
- w_value: bfloat16 [2048, 1024], P(None, 'tp'), may hold values from -0.125 to 0.125
- w_outgate: bfloat16 [2048, 1024], P(None, 'tp'), may hold values from -0.125 to 0.125
- w_igate: bfloat16 [2048, 4], P(None, 'tp'), may hold values from -0.125 to 0.125
- w_fgate: bfloat16 [2048, 4], P(None, 'tp'), may hold values from -0.125 to 0.125
- forget_bias: float32 [4], P('tp'), may hold values from -1 to 5
- w_out: bfloat16 [1024, 2048], P('tp'), may hold values from -0.1875 to 0.1875
- gain_mix: float32 [2048], replicated, may hold values from 0.1 to 1.9
- gain_moe: float32 [2048], replicated, may hold values from 0.1 to 1.9
- memory: float32 [64, 4, 256, 256], P('ep', 'tp'), may hold values from -0.4 to 0.4
- normalizer: float32 [64, 4, 256], P('ep', 'tp'), may hold values from -0.8 to 0.8
- stabilizer: float32 [64, 4], P('ep', 'tp'), may hold values from 0 to 2
- expert_gate: bfloat16 [8, 2048, 512], P('ep', None, 'tp'), may hold values from -0.125 to 0.125
- expert_up: bfloat16 [8, 2048, 512], P('ep', None, 'tp'), may hold values from -0.125 to 0.125
- expert_down: bfloat16 [8, 512, 2048], P('ep', 'tp'), may hold values from -1 to 1
- routes: int32 [64, 4], P('ep'), may hold values from 0 to 7, all different within a row; in each aligned block of 8 rows (0 to 7, 8 to 15, ...) at most 8 rows name the same one
- route_weight: float32 [64, 4], P('ep'), may hold values from 0.2 to 1
Outputs:
- output: bfloat16 [64, 2048], P('ep', 'tp')
- memory_next: float32 [64, 4, 256, 256], P('ep', 'tp')
- norm_next: float32 [64, 4, 256], P('ep', 'tp')
- stabilizer_next: float32 [64, 4], P('ep', 'tp')
Inputs may be any that keep to these rules, and one draw needn't show every extreme that they name: `routes`: each row names 4 different experts. Among the 8 rows of one device (aligned blocks), no expert is named more than 8 times, a bound that some block reaches.
All inputs are finite; a program needn't handle non-finite values.
Results may differ from a plain program's by a relative error of at most 0.029.
Values may be sent and summed in bfloat16 or wider, within the bound.
No kernel may reach another device: no remote copies, remote signals or barrier semaphores. Data moves between devices by JAX's collectives and lax.ppermute only.
A program may use at most 64 MiB of HBM per device.

v0:
```python
import math
import jax
import jax.numpy as jnp
from jax import lax
from jax.sharding import PartitionSpec as P


def layer_norm(row_data, gain_vec):
    values = row_data.astype(jnp.float32)
    row_mean = jnp.mean(values, -1, keepdims=True)
    centered = values - row_mean
    variance = jnp.mean(centered * centered, -1, keepdims=True)
    return centered * lax.rsqrt(variance + 1e-05) * gain_vec


def slot_targets(routes, experts, capacity):
    flat_routes = routes.reshape(-1)
    onehot = (flat_routes[:, None] == jnp.arange(experts, dtype=jnp.int32)[None, :]).astype(
        jnp.int32
    )
    before = jnp.cumsum(onehot, axis=0) - onehot
    slot_index = jnp.sum(before * onehot, axis=1)
    return flat_routes * capacity + slot_index


def shards(
    tokens,
    w_query,
    w_key,
    w_value,
    w_outgate,
    w_igate,
    w_fgate,
    forget_bias,
    w_out,
    gain_mix,
    gain_moe,
    memory,
    normalizer,
    stabilizer,
    expert_gate,
    expert_up,
    expert_down,
    routes,
    route_weight,
):
    seq_rows = tokens.shape[0]
    model_width = tokens.shape[1]
    head_count = memory.shape[1]
    head_size = memory.shape[2]
    head_cols = head_count * head_size
    normed = layer_norm(tokens, gain_mix).astype(jnp.bfloat16)
    gate_in = jnp.dot(normed, w_igate, preferred_element_type=jnp.float32)
    gate_forget = jnp.dot(normed, w_fgate, preferred_element_type=jnp.float32)
    weights = (w_query, w_key, w_value, w_outgate)
    projected = jnp.concatenate(
        [jnp.dot(normed, weight, preferred_element_type=jnp.float32) for weight in weights], axis=1
    )
    rounded = projected.astype(jnp.bfloat16).reshape(seq_rows, 4, head_count, head_size)
    queries = rounded[:, 0].astype(jnp.float32)
    keys_scaled = rounded[:, 1].astype(jnp.float32) / math.sqrt(head_size)
    values_rows = rounded[:, 2].astype(jnp.float32)
    out_gate = rounded[:, 3].astype(jnp.float32)
    log_forget = jax.nn.log_sigmoid(gate_forget + forget_bias)
    stabilizer_next = jnp.maximum(log_forget + stabilizer, gate_in)
    keep_rate = jnp.exp(log_forget + stabilizer - stabilizer_next)
    admit_rate = jnp.exp(gate_in - stabilizer_next)
    memory_next = (
        keep_rate[:, :, None, None] * memory
        + admit_rate[:, :, None, None] * keys_scaled[:, :, :, None] * values_rows[:, :, None, :]
    )
    norm_next = keep_rate[:, :, None] * normalizer + admit_rate[:, :, None] * keys_scaled
    numerator = jnp.einsum("shk,shkv->shv", queries, memory_next, precision=lax.Precision.HIGHEST)
    denominator = jnp.sum(queries * norm_next, axis=-1)
    readout = numerator / jnp.maximum(jnp.abs(denominator), jnp.exp(-stabilizer_next))[:, :, None]
    mixed = (jax.nn.sigmoid(out_gate) * readout).astype(jnp.bfloat16).reshape(seq_rows, head_cols)
    head_part = jnp.dot(mixed, w_out, preferred_element_type=jnp.float32).astype(jnp.bfloat16)
    summed = lax.psum(head_part, "tp").astype(jnp.float32)
    residual = tokens.astype(jnp.float32) + summed
    expert_in = layer_norm(residual, gain_moe).astype(jnp.bfloat16)
    top_count = routes.shape[1]
    local_experts = expert_gate.shape[0]
    expert_count = local_experts * lax.axis_size("ep")
    capacity = max(2, 2 * seq_rows * top_count // expert_count)
    target = slot_targets(routes, expert_count, capacity)
    outbound = (
        jnp.zeros((expert_count * capacity, model_width), jnp.bfloat16)
        .at[target]
        .set(jnp.repeat(expert_in, top_count, axis=0))
    )
    outbound = outbound.reshape(expert_count, capacity, model_width)
    quarter = model_width // lax.axis_size("tp")
    arrived = lax.all_to_all(outbound, "ep", split_axis=0, concat_axis=0, tiled=True)
    slot_count = arrived.shape[1]
    grouped = arrived.reshape(-1, local_experts, slot_count, model_width)
    gate_part = jnp.einsum(
        "aecd,edf->aecf", grouped, expert_gate, preferred_element_type=jnp.float32
    )
    up_part = jnp.einsum("aecd,edf->aecf", grouped, expert_up, preferred_element_type=jnp.float32)
    hidden = (jax.nn.silu(gate_part) * up_part).astype(jnp.bfloat16)
    partial_value, slot_count = (
        jnp.einsum("aecf,efd->aecd", hidden, expert_down, preferred_element_type=jnp.float32),
        slot_count,
    )
    reduced = lax.psum_scatter(partial_value, "tp", scatter_dimension=3, tiled=True).astype(
        jnp.bfloat16
    )
    reduced = reduced.reshape(-1, slot_count, reduced.shape[3])
    returned = lax.all_to_all(reduced, "ep", split_axis=0, concat_axis=0, tiled=True)
    picked = jnp.take(returned.reshape(expert_count * capacity, quarter), target, axis=0).reshape(
        seq_rows, top_count, quarter
    )
    combined = jnp.sum(route_weight[:, :, None] * picked.astype(jnp.float32), axis=1)
    own_cols = lax.dynamic_slice_in_dim(residual, lax.axis_index("tp") * quarter, quarter, 1)
    output = (own_cols + combined).astype(jnp.bfloat16)
    return (output, memory_next, norm_next, stabilizer_next)


def solution(mesh):
    return jax.shard_map(
        shards,
        mesh=mesh,
        in_specs=(
            P("ep", None),
            P(None, "tp"),
            P(None, "tp"),
            P(None, "tp"),
            P(None, "tp"),
            P(None, "tp"),
            P(None, "tp"),
            P("tp"),
            P("tp", None),
            P(),
            P(),
            P("ep", "tp", None, None),
            P("ep", "tp", None),
            P("ep", "tp"),
            P("ep", None, "tp"),
            P("ep", None, "tp"),
            P("ep", "tp", None),
            P("ep", None),
            P("ep", None),
        ),
        out_specs=(P("ep", "tp"), P("ep", "tp", None, None), P("ep", "tp", None), P("ep", "tp")),
        check_vma=False,
    )
```

profile of v0, /device:TPU:0, one launch (start us, length us, event | category | flops | bytes accessed | tf_op | source)
XLA Modules:
  0.0 94.1 jit_solution(10027938302184542748)
XLA Ops:
  7.2 0.9 copy.30
  8.2 1.0 %convert_reduce_fusion = f32[8]{0:T(128)S(1)} fusion(bf16[8,2048]{1,0:T(8,128)(2,1)} %param.19), kind=kLoop, calls=%fused_computation.36 | loop fusion | flops 32760 | bytes 32800 | tf_op jit(solution)/shard_map/reduce_sum | solution.py:10
  9.3 1.0 %fusion.24 = f32[8]{0:T(128)S(1)} fusion(bf16[8,2048]{1,0:T(8,128)(2,1)} %param.19, f32[8]{0:T(128)S(1)} %broadcast_multiply_fusion.3), kind=kLoop, calls=%fused_computation.39 | loop fusion | flops 65528 | bytes 32832 | tf_op jit(solution)/shard_map/reduce_sum | solution.py:12
  10.9 0.8 fusion.26
  11.7 0.8 convolution_bitcast_fusion.3
  12.6 0.8 exponential_bitcast_fusion
  13.4 1.5 %fusion.5 = f32[8,256]{1,0:T(8,128)S(1)} fusion(bf16[8,2048]{1,0:T(8,128)(2,1)S(1)} %fusion.26, bf16[2048,256]{1,0:T(8,128)(2,1)} %param.22), kind=kOutput, calls=%fused_computation.13 | convolution fusion | flops 8392704 | bytes 1089536 | tf_op jit(solution)/shard_map/dot_general | solution.py:57
  14.9 1.4 %broadcast_multiply_fusion = (f32[8,256]{1,0:T(8,128)S(1)}, f32[8,256]{1,0:T(8,128)S(1)}) fusion(f32[8]{0:T(128)S(1)} %multiply_bitcast_fusion, bf16[8,2048]{1,0:T(8,128)(2,1)S(1)} %fusion.26, bf16[2048,256]{1,0:T(8,128)(2,1)} %param.21), kind=kOutput, calls=%fused_computation.68 | convolution fusion | flops 8394752 | bytes 1097760 | tf_op jit(solution)/shard_map/dot_general | solution.py:57
  16.4 0.4 fusion.34
  16.8 0.5 multiply_add_fusion
  17.3 0.8 fusion
  18.1 2.0 %convolution_convert_fusion = bf16[8,2048]{1,0:T(8,128)(2,1)S(1)} fusion(bf16[256,2048]{1,0:T(8,128)(2,1)S(1)} %copy-done, bf16[8,2048]{1,0:T(8,128)(2,1)S(1)} %fusion.26, bf16[2048,256]{1,0:T(8,128)(2,1)} %param.23, f32[8,1,256]{2,1,0:T(1,128)S(1)} %fusion, f32[8]{0:T(128)S(1)} %fusion.42), kind=kOutput, calls=%fused_computation.3 | convolution fusion | flops 16809984 | bytes 2170912 | tf_op jit(solution)/shard_map/dot_general | solution.py:77
  20.1 12.9 %psum.7 = bf16[8,2048]{1,0:T(8,128)(2,1)S(1)} all-reduce(bf16[8,2048]{1,0:T(8,128)(2,1)S(1)} %convolution_convert_fusion), channel_id=1, replica_groups=mesh['ep'=8,'tp'=4] {'tp'}, use_global_device_ids=true, to_apply=%region_3.4 | all-reduce | flops 16384 | bytes 65536 | tf_op jit(solution)/shard_map/psum | solution.py:78
  34.0 0.9 scatter_custom_fusion
  34.9 13.9 %all_to_all.10 = bf16[8,8,2048]{2,1,0:T(8,128)(2,1)S(1)} all-to-all(bf16[8,8,2048]{2,1,0:T(8,128)(2,1)S(1)} %bitcast.115), channel_id=1, replica_groups=mesh['ep'=8,'tp'=4] {'ep'}, dimensions={0} | all-to-all | bytes 524288 | tf_op jit(solution)/shard_map/all_to_all | solution.py:93
  48.7 1.3 %convolution_bitcast_fusion.2 = f32[8,1,8,128]{3,2,0,1:T(8,128)S(1)} fusion(bf16[8,8,2048]{2,1,0:T(8,128)(2,1)S(1)} %all_to_all.10, bf16[1,2048,128]{2,1,0:T(8,128)(2,1)} %param.33), kind=kOutput, calls=%fused_computation.9 | convolution fusion | flops 33554432 | bytes 819200 | tf_op jit(solution)/shard_map/aecd,edf->aecf/dot_general | solution.py:96
  50.0 1.2 %convolution_bitcast_fusion = f32[8,1,8,2048]{3,2,0,1:T(8,128)} fusion(bf16[8,8,2048]{2,1,0:T(8,128)(2,1)S(1)} %all_to_all.10, bf16[1,128,2048]{2,1,0:T(8,128)(2,1)S(1)} %copy-done.5, bf16[1,2048,128]{2,1,0:T(8,128)(2,1)S(1)} %copy-done.6, f32[8,1,8,128]{3,2,0,1:T(8,128)S(1)} %convolution_bitcast_fusion.2), kind=kOutput, calls=%fused_computation.2 | convolution fusion | flops 67158016 | bytes 1867776 | tf_op jit(solution)/shard_map/aecf,efd->aecd/dot_general | solution.py:102
  51.3 20.7 %reduce-scatter.2.cloned.1.call-done = f32[8,1,8,512]{3,2,0,1:T(8,128)} async-done(((f32[8,1,8,2048]{3,2,0,1:T(8,128)}), f32[8,1,8,512]{3,2,0,1:T(8,128)}) %reduce-scatter.2.cloned.1.call-update) | async-done | bytes 131088 | tf_op jit(solution)/shard_map/reduce_scatter | solution.py:105
  72.0 1.5 %convert_bitcast_fusion = bf16[8,8,512]{2,1,0:T(8,128)(2,1)} fusion(f32[8,1,8,512]{3,2,0,1:T(8,128)} %reduce-scatter.2.cloned.1.call-done), kind=kLoop, calls=%fused_computation.43 | loop fusion | flops 32768 | bytes 196608 | tf_op jit(solution)/shard_map/reshape | solution.py:108
  73.5 5.5 %all-to-all-start.1 = ((bf16[8,8,512]{2,1,0:T(8,128)(2,1)}), bf16[8,8,512]{2,1,0:T(8,128)(2,1)S(1)}, u32[]{:S(2)}, u32[]{:S(2)}) async-start(bf16[8,8,512]{2,1,0:T(8,128)(2,1)} %convert_bitcast_fusion), calls=%async_computation.2 | async-start | bytes 131072 | tf_op jit(solution)/shard_map/all_to_all | solution.py:109
  79.1 0.6 copy.32
  79.7 6.2 %all-to-all-done.1 = bf16[8,8,512]{2,1,0:T(8,128)(2,1)S(1)} async-done(((bf16[8,8,512]{2,1,0:T(8,128)(2,1)}), bf16[8,8,512]{2,1,0:T(8,128)(2,1)S(1)}, u32[]{:S(2)}, u32[]{:S(2)}) %all-to-all-start.1) | async-done | bytes 65568 | tf_op jit(solution)/shard_map/all_to_all | solution.py:109
  85.9 0.6 gather_fusion
  86.7 0.6 add_convert_fusion
  (48 shorter events, 1.5 us)
Async XLA Ops:
  7.2 11.0 %copy-start = (bf16[256,2048]{1,0:T(8,128)(2,1)S(1)}, bf16[256,2048]{1,0:T(8,128)(2,1)}, u32[]{:S(2)}) copy-start(bf16[256,2048]{1,0:T(8,128)(2,1)} %param.27) | copy-start | bytes 3145732
  7.2 9.2 %copy-start.4 = (bf16[2048,256]{1,0:T(8,128)(2,1)S(1)}, bf16[2048,256]{1,0:T(8,128)(2,1)}, u32[]{:S(2)}) copy-start(bf16[2048,256]{1,0:T(8,128)(2,1)} %param.20) | copy-start | bytes 3145732
  7.2 9.2 %copy-start.7 = (f32[8,1,256]{2,1,0:T(1,128)S(1)}, f32[8,1,256]{2,1,0:T(1,128)}, u32[]{:S(2)}) copy-start(f32[8,1,256]{2,1,0:T(1,128)} %param.31) | copy-start | bytes 24580
  7.2 64.8 %reduce-scatter.2.cloned.1.call-start = ((), (), s32[]{:S(2)}) async-start(), calls=%async_computation.3 | async-start | bytes 655360 | tf_op jit(solution)/shard_map/reduce_scatter | solution.py:105
  8.2 8.6 %copy-start.2 = (f32[8,1,256,256]{3,2,1,0:T(8,128)S(1)}, f32[8,1,256,256]{3,2,1,0:T(8,128)}, u32[]{:S(2)}) copy-start(f32[8,1,256,256]{3,2,1,0:T(8,128)} %param.30) | copy-start | bytes 6291460
  13.4 3.8 %copy-start.10 = (f32[8,1]{0,1:T(1,128)}, f32[8,1]{0,1:T(1,128)S(1)}, u32[]{:S(2)}) copy-start(f32[8,1]{0,1:T(1,128)S(1)} %get-tuple-element.15) | copy-start | bytes 100
  17.3 2.8 %copy-start.1 = (f32[8,1,256,256]{3,2,1,0:T(8,128)}, f32[8,1,256,256]{3,2,1,0:T(8,128)S(1)}, u32[]{:S(2)}) copy-start(f32[8,1,256,256]{3,2,1,0:T(8,128)S(1)} %multiply_add_fusion) | copy-start | bytes 6291460
  17.3 15.7 %copy-start.3 = (bf16[8,2048]{1,0:T(8,128)(2,1)S(1)}, bf16[8,2048]{1,0:T(8,128)(2,1)}, u32[]{:S(2)}) copy-start(bf16[8,2048]{1,0:T(8,128)(2,1)} %param.19) | copy-start | bytes 98308
  17.3 16.1 %copy-start.8 = (f32[2048]{0:T(1024)S(1)}, f32[2048]{0:T(1024)}, u32[]{:S(2)}) copy-start(f32[2048]{0:T(1024)} %param.29) | copy-start | bytes 24580
  33.0 17.0 %copy-start.5 = (bf16[1,128,2048]{2,1,0:T(8,128)(2,1)S(1)}, bf16[1,128,2048]{2,1,0:T(8,128)(2,1)}, u32[]{:S(2)}) copy-start(bf16[1,128,2048]{2,1,0:T(8,128)(2,1)} %param.35) | copy-start | bytes 1572868
  33.0 17.0 %copy-start.6 = (bf16[1,2048,128]{2,1,0:T(8,128)(2,1)S(1)}, bf16[1,2048,128]{2,1,0:T(8,128)(2,1)}, u32[]{:S(2)}) copy-start(bf16[1,2048,128]{2,1,0:T(8,128)(2,1)} %param.34) | copy-start | bytes 1572868
  34.9 44.2 %copy-start.9 = (f32[8,4]{0,1:T(4,128)S(1)}, f32[8,4]{0,1:T(4,128)}, u32[]{:S(2)}) copy-start(f32[8,4]{0,1:T(4,128)} %param.37) | copy-start | bytes 388
  73.5 12.4 %all-to-all-start.1 = ((bf16[8,8,512]{2,1,0:T(8,128)(2,1)}), bf16[8,8,512]{2,1,0:T(8,128)(2,1)S(1)}, u32[]{:S(2)}, u32[]{:S(2)}) async-start(bf16[8,8,512]{2,1,0:T(8,128)(2,1)} %convert_bitcast_fusion), calls=%async_computation.2 | async-start | bytes 131072 | tf_op jit(solution)/shard_map/all_to_all | solution.py:109
Sparse Core Ops, SparseCore 0:
  51.3 20.5 reduce-scatter.1
where the time goes:
time: 94.8 us; the launch traced here: 94.1 us
  waiting for transfers between devices  26.9 us (28%)
  blocking collectives  26.8 us (28%)
  between operations  14.9 us (16%)
  matrix products  10.2 us (11%)
  other arithmetic  6.35 us (7%)
  starting transfers between devices  5.55 us (6%)
  local copies, waits for them, and re-layouts  3.52 us (4%)
    reduce_scatter x1, waiting for transfers between devices, shards(): lax.psum_scatter(partial_value, 'tp', scatter_dimension=3, tiled=True)  20.7 us
    all_to_all x1, blocking collectives, shards(): lax.all_to_all(outbound, 'ep', split_axis=0, concat_axis=0, tiled=True)  13.9 us
    psum x1, blocking collectives, shards(): summed = lax.psum(head_part, 'tp').astype(jnp.float32)  12.9 us
    all_to_all x1, waiting for transfers between devices, shards(): lax.all_to_all(reduced, 'ep', split_axis=0, concat_axis=0, tiled=True)  6.19 us
    all_to_all x1, starting transfers between devices, shards(): lax.all_to_all(reduced, 'ep', split_axis=0, concat_axis=0, tiled=True)  5.52 us
    dot_general x3, matrix products, shards(): jnp.dot(normed, weight, preferred_element_type=jnp.float32)  3.27 us
    dot_general x1, matrix products, shards(): jnp.dot(mixed, w_out, preferred_element_type=jnp.float32)  1.96 us
  transfers between devices with their start and end apart: 2, of which 2 were waited for; matrix products, arithmetic and copies ran while one was open for 1% of the time, Pallas kernels for 0%

commit v1 on v0

--- a/solution.py
+++ b/solution.py
@@ -3,6 +3,12 @@
 import jax.numpy as jnp
 from jax import lax
 from jax.sharding import PartitionSpec as P
+
+
+def add_all(array, axis):
+    terms = lax.all_gather(array, axis, axis=0, tiled=False)
+    total = terms.sum(axis=0)
+    return total
 
 
 def layer_norm(row_data, gain_vec):
@@ -75,7 +81,7 @@
     readout = numerator / jnp.maximum(jnp.abs(denominator), jnp.exp(-stabilizer_next))[:, :, None]
     mixed = (jax.nn.sigmoid(out_gate) * readout).astype(jnp.bfloat16).reshape(seq_rows, head_cols)
     head_part = jnp.dot(mixed, w_out, preferred_element_type=jnp.float32).astype(jnp.bfloat16)
-    summed = lax.psum(head_part, "tp").astype(jnp.float32)
+    summed = add_all(head_part, "tp").astype(jnp.float32)
     residual = tokens.astype(jnp.float32) + summed
     expert_in = layer_norm(residual, gain_moe).astype(jnp.bfloat16)
     top_count = routes.shape[1]

time: 94.8 us -> 90 us (0.949)
  blocking collectives: 26.8 us -> 22 us
    psum x1 -> x0, blocking collectives: 12.9 us -> none  [shards(): summed = lax.psum(head_part, 'tp').astype(jnp.float32)]
    all_gather x0 -> x1, blocking collectives: none -> 6.51 us  [add_all(): terms = lax.all_gather(array, axis, axis=0, tiled=False)]
    all_to_all x1, blocking collectives: 13.9 us -> 15.4 us  [shards(): lax.all_to_all(outbound, 'ep', split_axis=0, concat_axis=0, tiled=True)]
where the time goes in v1:
time: 90 us; the launch traced here: 89.4 us
  waiting for transfers between devices  26.9 us (30%)
  blocking collectives  22 us (24%)
  between operations  14.9 us (17%)
  matrix products  10.2 us (11%)
  other arithmetic  6.37 us (7%)
  starting transfers between devices  5.56 us (6%)
  local copies, waits for them, and re-layouts  3.51 us (4%)
    reduce_scatter x1, waiting for transfers between devices, shards(): lax.psum_scatter(partial_value, 'tp', scatter_dimension=3, tiled=True)  20.7 us
    all_to_all x1, blocking collectives, shards(): lax.all_to_all(outbound, 'ep', split_axis=0, concat_axis=0, tiled=True)  15.4 us
    all_gather x1, blocking collectives, add_all(): terms = lax.all_gather(array, axis, axis=0, tiled=False)  6.51 us
    all_to_all x1, waiting for transfers between devices, shards(): lax.all_to_all(reduced, 'ep', split_axis=0, concat_axis=0, tiled=True)  6.19 us
    all_to_all x1, starting transfers between devices, shards(): lax.all_to_all(reduced, 'ep', split_axis=0, concat_axis=0, tiled=True)  5.52 us
    dot_general x3, matrix products, shards(): jnp.dot(normed, weight, preferred_element_type=jnp.float32)  3.27 us
    dot_general x1, matrix products, shards(): jnp.dot(mixed, w_out, preferred_element_type=jnp.float32)  1.96 us
  transfers between devices with their start and end apart: 2, of which 2 were waited for; matrix products, arithmetic and copies ran while one was open for 1% of the time, Pallas kernels for 0%

profile of v1, /device:TPU:0, one launch (start us, length us, event | category | flops | bytes accessed | tf_op | source)
XLA Modules:
  0.0 89.4 jit_solution(1957538643711558572)
XLA Ops:
  7.2 0.9 copy.30
  8.2 1.0 %convert_reduce_fusion = f32[8]{0:T(128)S(1)} fusion(bf16[8,2048]{1,0:T(8,128)(2,1)} %param.19), kind=kLoop, calls=%fused_computation.37 | loop fusion | flops 32760 | bytes 32800 | tf_op jit(solution)/shard_map/reduce_sum | solution.py:16
  9.3 1.0 %fusion.24 = f32[8]{0:T(128)S(1)} fusion(bf16[8,2048]{1,0:T(8,128)(2,1)} %param.19, f32[8]{0:T(128)S(1)} %broadcast_multiply_fusion.3), kind=kLoop, calls=%fused_computation.40 | loop fusion | flops 65528 | bytes 32832 | tf_op jit(solution)/shard_map/reduce_sum | solution.py:18
  10.9 0.8 fusion.26
  11.7 0.8 convolution_bitcast_fusion.3
  12.6 0.8 exponential_bitcast_fusion
  13.4 1.5 %fusion.5 = f32[8,256]{1,0:T(8,128)S(1)} fusion(bf16[8,2048]{1,0:T(8,128)(2,1)S(1)} %fusion.26, bf16[2048,256]{1,0:T(8,128)(2,1)} %param.22), kind=kOutput, calls=%fused_computation.13 | convolution fusion | flops 8392704 | bytes 1089536 | tf_op jit(solution)/shard_map/dot_general | solution.py:63
  14.9 1.4 %broadcast_multiply_fusion = (f32[8,256]{1,0:T(8,128)S(1)}, f32[8,256]{1,0:T(8,128)S(1)}) fusion(f32[8]{0:T(128)S(1)} %multiply_bitcast_fusion, bf16[8,2048]{1,0:T(8,128)(2,1)S(1)} %fusion.26, bf16[2048,256]{1,0:T(8,128)(2,1)} %param.21), kind=kOutput, calls=%fused_computation.69 | convolution fusion | flops 8394752 | bytes 1097760 | tf_op jit(solution)/shard_map/dot_general | solution.py:63
  16.4 0.4 fusion.34
  16.8 0.5 multiply_add_fusion
  17.3 0.8 fusion
  18.1 2.0 %convolution_convert_fusion = bf16[8,2048]{1,0:T(8,128)(2,1)S(1)} fusion(bf16[256,2048]{1,0:T(8,128)(2,1)S(1)} %copy-done, bf16[8,2048]{1,0:T(8,128)(2,1)S(1)} %fusion.26, bf16[2048,256]{1,0:T(8,128)(2,1)} %param.23, f32[8,1,256]{2,1,0:T(1,128)S(1)} %fusion, f32[8]{0:T(128)S(1)} %fusion.42), kind=kOutput, calls=%fused_computation.3 | convolution fusion | flops 16809984 | bytes 2170912 | tf_op jit(solution)/shard_map/dot_general | solution.py:83
  20.1 6.5 %all-gather = bf16[32,2048]{1,0:T(8,128)(2,1)S(1)} all-gather(bf16[8,2048]{1,0:T(8,128)(2,1)S(1)} %convolution_convert_fusion), channel_id=2, replica_groups=mesh['ep'=8,'tp'=4] {'tp'}, dimensions={0}, use_global_device_ids=true | all-gather | bytes 163840 | tf_op jit(solution)/shard_map/all_gather | solution.py:9
  27.6 0.9 scatter_custom_fusion
  28.5 15.4 %all_to_all.10 = bf16[8,8,2048]{2,1,0:T(8,128)(2,1)S(1)} all-to-all(bf16[8,8,2048]{2,1,0:T(8,128)(2,1)S(1)} %bitcast.117), channel_id=1, replica_groups=mesh['ep'=8,'tp'=4] {'ep'}, dimensions={0} | all-to-all | bytes 524288 | tf_op jit(solution)/shard_map/all_to_all | solution.py:99
  43.9 1.3 %convolution_bitcast_fusion.2 = f32[8,1,8,128]{3,2,0,1:T(8,128)S(1)} fusion(bf16[8,8,2048]{2,1,0:T(8,128)(2,1)S(1)} %all_to_all.10, bf16[1,2048,128]{2,1,0:T(8,128)(2,1)} %param.33), kind=kOutput, calls=%fused_computation.9 | convolution fusion | flops 33554432 | bytes 819200 | tf_op jit(solution)/shard_map/aecd,edf->aecf/dot_general | solution.py:102
  45.2 1.2 %convolution_bitcast_fusion = f32[8,1,8,2048]{3,2,0,1:T(8,128)} fusion(bf16[8,8,2048]{2,1,0:T(8,128)(2,1)S(1)} %all_to_all.10, bf16[1,128,2048]{2,1,0:T(8,128)(2,1)S(1)} %copy-done.5, bf16[1,2048,128]{2,1,0:T(8,128)(2,1)S(1)} %copy-done.6, f32[8,1,8,128]{3,2,0,1:T(8,128)S(1)} %convolution_bitcast_fusion.2), kind=kOutput, calls=%fused_computation.2 | convolution fusion | flops 67158016 | bytes 1867776 | tf_op jit(solution)/shard_map/aecf,efd->aecd/dot_general | solution.py:108
  46.5 20.7 %reduce-scatter.2.cloned.1.call-done = f32[8,1,8,512]{3,2,0,1:T(8,128)} async-done(((f32[8,1,8,2048]{3,2,0,1:T(8,128)}), f32[8,1,8,512]{3,2,0,1:T(8,128)}) %reduce-scatter.2.cloned.1.call-update) | async-done | bytes 131088 | tf_op jit(solution)/shard_map/reduce_scatter | solution.py:111
  67.2 1.5 %convert_bitcast_fusion = bf16[8,8,512]{2,1,0:T(8,128)(2,1)} fusion(f32[8,1,8,512]{3,2,0,1:T(8,128)} %reduce-scatter.2.cloned.1.call-done), kind=kLoop, calls=%fused_computation.44 | loop fusion | flops 32768 | bytes 196608 | tf_op jit(solution)/shard_map/reshape | solution.py:114
  68.7 5.5 %all-to-all-start.1 = ((bf16[8,8,512]{2,1,0:T(8,128)(2,1)}), bf16[8,8,512]{2,1,0:T(8,128)(2,1)S(1)}, u32[]{:S(2)}, u32[]{:S(2)}) async-start(bf16[8,8,512]{2,1,0:T(8,128)(2,1)} %convert_bitcast_fusion), calls=%async_computation.2 | async-start | bytes 131072 | tf_op jit(solution)/shard_map/all_to_all | solution.py:115
  74.4 0.6 copy.32
  75.0 6.2 %all-to-all-done.1 = bf16[8,8,512]{2,1,0:T(8,128)(2,1)S(1)} async-done(((bf16[8,8,512]{2,1,0:T(8,128)(2,1)}), bf16[8,8,512]{2,1,0:T(8,128)(2,1)S(1)}, u32[]{:S(2)}, u32[]{:S(2)}) %all-to-all-start.1) | async-done | bytes 65568 | tf_op jit(solution)/shard_map/all_to_all | solution.py:115
  81.2 0.6 gather_fusion
  81.9 0.6 add_convert_fusion
  (49 shorter events, 1.5 us)
Async XLA Ops:
  7.2 11.0 %copy-start = (bf16[256,2048]{1,0:T(8,128)(2,1)S(1)}, bf16[256,2048]{1,0:T(8,128)(2,1)}, u32[]{:S(2)}) copy-start(bf16[256,2048]{1,0:T(8,128)(2,1)} %param.27) | copy-start | bytes 3145732
  7.2 9.2 %copy-start.4 = (bf16[2048,256]{1,0:T(8,128)(2,1)S(1)}, bf16[2048,256]{1,0:T(8,128)(2,1)}, u32[]{:S(2)}) copy-start(bf16[2048,256]{1,0:T(8,128)(2,1)} %param.20) | copy-start | bytes 3145732
  7.2 9.2 %copy-start.7 = (f32[8,1,256]{2,1,0:T(1,128)S(1)}, f32[8,1,256]{2,1,0:T(1,128)}, u32[]{:S(2)}) copy-start(f32[8,1,256]{2,1,0:T(1,128)} %param.31) | copy-start | bytes 24580
  7.2 60.0 %reduce-scatter.2.cloned.1.call-start = ((), (), s32[]{:S(2)}) async-start(), calls=%async_computation.3 | async-start | bytes 655360 | tf_op jit(solution)/shard_map/reduce_scatter | solution.py:111
  8.2 8.6 %copy-start.2 = (f32[8,1,256,256]{3,2,1,0:T(8,128)S(1)}, f32[8,1,256,256]{3,2,1,0:T(8,128)}, u32[]{:S(2)}) copy-start(f32[8,1,256,256]{3,2,1,0:T(8,128)} %param.30) | copy-start | bytes 6291460
  13.4 3.8 %copy-start.10 = (f32[8,1]{0,1:T(1,128)}, f32[8,1]{0,1:T(1,128)S(1)}, u32[]{:S(2)}) copy-start(f32[8,1]{0,1:T(1,128)S(1)} %get-tuple-element.15) | copy-start | bytes 100
  17.3 2.8 %copy-start.1 = (f32[8,1,256,256]{3,2,1,0:T(8,128)}, f32[8,1,256,256]{3,2,1,0:T(8,128)S(1)}, u32[]{:S(2)}) copy-start(f32[8,1,256,256]{3,2,1,0:T(8,128)S(1)} %multiply_add_fusion) | copy-start | bytes 6291460
  17.3 9.3 %copy-start.3 = (bf16[8,2048]{1,0:T(8,128)(2,1)S(1)}, bf16[8,2048]{1,0:T(8,128)(2,1)}, u32[]{:S(2)}) copy-start(bf16[8,2048]{1,0:T(8,128)(2,1)} %param.19) | copy-start | bytes 98308
  17.3 9.7 %copy-start.8 = (f32[2048]{0:T(1024)S(1)}, f32[2048]{0:T(1024)}, u32[]{:S(2)}) copy-start(f32[2048]{0:T(1024)} %param.29) | copy-start | bytes 24580
  26.6 18.6 %copy-start.5 = (bf16[1,128,2048]{2,1,0:T(8,128)(2,1)S(1)}, bf16[1,128,2048]{2,1,0:T(8,128)(2,1)}, u32[]{:S(2)}) copy-start(bf16[1,128,2048]{2,1,0:T(8,128)(2,1)} %param.35) | copy-start | bytes 1572868
  26.6 18.6 %copy-start.6 = (bf16[1,2048,128]{2,1,0:T(8,128)(2,1)S(1)}, bf16[1,2048,128]{2,1,0:T(8,128)(2,1)}, u32[]{:S(2)}) copy-start(bf16[1,2048,128]{2,1,0:T(8,128)(2,1)} %param.34) | copy-start | bytes 1572868
  28.5 45.8 %copy-start.9 = (f32[8,4]{0,1:T(4,128)S(1)}, f32[8,4]{0,1:T(4,128)}, u32[]{:S(2)}) copy-start(f32[8,4]{0,1:T(4,128)} %param.37) | copy-start | bytes 388
  68.7 12.4 %all-to-all-start.1 = ((bf16[8,8,512]{2,1,0:T(8,128)(2,1)}), bf16[8,8,512]{2,1,0:T(8,128)(2,1)S(1)}, u32[]{:S(2)}, u32[]{:S(2)}) async-start(bf16[8,8,512]{2,1,0:T(8,128)(2,1)} %convert_bitcast_fusion), calls=%async_computation.2 | async-start | bytes 131072 | tf_op jit(solution)/shard_map/all_to_all | solution.py:115
Sparse Core Ops, SparseCore 0:
  46.5 20.6 reduce-scatter.1
